TPU v7x, 32 devices: a whole 2x2x4 slice. The times are simulated.
32 devices in a mesh: sp: 8 (over z, y), tp: 4 (over x, core).
Axes of the slice: x: 2, y: 2, z: 4, core: 2. Of those that a mesh axis runs over, the one named last changes fastest.
Arguments:
- hidden_state: bfloat16 [1024, 2048], P('sp'), may hold values from -6 to 6
- out_grad: bfloat16 [1024, 2048], P('sp'), may hold values from -8 to 8
- routes: int32 [1024, 2], P('sp'), may hold values from 0 to 3, all different within a row; in each aligned block of 128 rows (0 to 127, 128 to 255, ...) at most 96 rows name the same one
- route_weights: float32 [1024, 2], P('sp'), may hold values from 0.25 to 1
- w_gate: bfloat16 [8, 2048, 1792], P('sp', None, 'tp'), may hold values from -0.125 to 0.125
- w_up: bfloat16 [8, 2048, 1792], P('sp', None, 'tp'), may hold values from -0.125 to 0.125
- w_down: bfloat16 [8, 1792, 2048], P('sp', 'tp'), may hold values from -0.09375 to 0.09375
- value: bfloat16 [1024, 512], P('sp', 'tp'), may hold values from -6 to 6
- gate_in: bfloat16 [1024, 512], P('sp', 'tp'), may hold values from -6 to 6
- normed: bfloat16 [1024, 512], P('sp', 'tp'), may hold values from -24 to 24
- inv_std: float32 [1024], P('sp'), may hold values from 0.5 to 2
- norm_gain: float32 [512], P('tp'), may hold values from 0.1 to 1.9
- taps: float32 [31, 512], P(None, 'tp'), may hold values from -1 to 1
- w_proj: bfloat16 [2048, 512], P(None, 'tp'), may hold values from -0.25 to 0.25
Outputs:
- w_gate_grad: bfloat16 [8, 2048, 1792], P('sp', None, 'tp')
- w_up_grad: bfloat16 [8, 2048, 1792], P('sp', None, 'tp')
- w_down_grad: bfloat16 [8, 1792, 2048], P('sp', 'tp')
- stream_grad: bfloat16 [1024, 2048], P('sp', 'tp')
- proj_grad: float32 [2048, 512], P('sp', 'tp')
- value_grad: bfloat16 [1024, 512], P('sp', 'tp')
- gate_in_grad: bfloat16 [1024, 512], P('sp', 'tp')
Inputs may be any that keep to these rules, and one draw needn't show every extreme that they name: `routes`: among the choices of one device's tokens no expert is named more than 96 times, a bound that some block reaches on some device; a token's choices differ.
All inputs are finite; a program needn't handle non-finite values.
Results may differ from a plain program's by a relative error of at most 0.0057.
Values may be sent and summed in bfloat16 or wider, within the bound.
A program may use at most 128 MiB of HBM per device.

v0:
```python
import jax
import jax.numpy as jnp
from jax import lax
from jax.sharding import PartitionSpec as P

D_CH = 512
KSIZE = 31
GROUP = 2


def passed_along(value, axis, by):
    peers = lax.axis_size(axis)
    pairs = [(i, i + by) for i in range(peers) if 0 <= i + by < peers]
    return lax.ppermute(value, axis, pairs)


def expert_backward(in_rows, in_cots, gate_slice, up_slice, down_slice):
    pre_gate = jnp.dot(in_rows, gate_slice, preferred_element_type=jnp.float32)
    pre_up = jnp.dot(in_rows, up_slice, preferred_element_type=jnp.float32)
    gate_sig = jax.nn.sigmoid(pre_gate)
    silu_gate = pre_gate * gate_sig
    act_rows = (silu_gate * pre_up).astype(jnp.bfloat16)
    act_grad = lax.dot_general(
        in_cots, down_slice, (((1,), (1,)), ((), ())), preferred_element_type=jnp.float32
    )
    gate_grad = (act_grad * pre_up * gate_sig * (1.0 + pre_gate * (1.0 - gate_sig))).astype(
        jnp.bfloat16
    )
    up_grad = (act_grad * silu_gate).astype(jnp.bfloat16)
    down_grad = lax.dot_general(
        act_rows, in_cots, (((0,), (0,)), ((), ())), preferred_element_type=jnp.float32
    )
    gate_wgrad = lax.dot_general(
        in_rows, gate_grad, (((0,), (0,)), ((), ())), preferred_element_type=jnp.float32
    )
    up_wgrad = lax.dot_general(
        in_rows, up_grad, (((0,), (0,)), ((), ())), preferred_element_type=jnp.float32
    )
    row_grad = lax.dot_general(
        gate_grad, gate_slice, (((1,), (1,)), ((), ())), preferred_element_type=jnp.float32
    )
    row_grad = row_grad + lax.dot_general(
        up_grad, up_slice, (((1,), (1,)), ((), ())), preferred_element_type=jnp.float32
    )
    return (
        gate_wgrad.astype(jnp.bfloat16),
        up_wgrad.astype(jnp.bfloat16),
        down_grad.astype(jnp.bfloat16),
        row_grad,
    )


def slot_table(routes, route_weights, experts, capacity):
    tok_rows, top_k = routes.shape
    flat_routes = routes.reshape(-1)
    onehot = (flat_routes[:, None] == jnp.arange(experts, dtype=jnp.int32)[None, :]).astype(
        jnp.int32
    )
    before = jnp.cumsum(onehot, axis=0) - onehot
    slot_index = jnp.sum(before * onehot, axis=1)
    slot_place = flat_routes * capacity + slot_index
    row_owner = jnp.arange(tok_rows * top_k, dtype=jnp.int32) // top_k
    row_table = jnp.full((experts * capacity,), tok_rows, jnp.int32).at[slot_place].set(row_owner)
    row_scale = (
        jnp.zeros((experts * capacity,), jnp.float32).at[slot_place].set(route_weights.reshape(-1))
    )
    return (slot_place, row_table, row_scale)


def pack_rows(states, cot_pad, row_table, row_scale, experts, capacity):
    columns = states.shape[1]
    sent_rows = jnp.take(states, row_table, axis=0)
    sent_cots = (
        jnp.take(cot_pad, row_table, axis=0).astype(jnp.float32) * row_scale[:, None]
    ).astype(jnp.bfloat16)
    copies = (experts, GROUP, capacity, columns)
    sent_rows = jnp.broadcast_to(sent_rows.reshape(experts, 1, capacity, columns), copies).reshape(
        experts * GROUP * capacity, columns
    )
    sent_cots = jnp.broadcast_to(sent_cots.reshape(experts, 1, capacity, columns), copies).reshape(
        experts * GROUP * capacity, columns
    )
    return (sent_rows, sent_cots)


def on_device(
    hidden_state,
    out_grad,
    routes,
    route_weights,
    w_gate,
    w_up,
    w_down,
    value,
    gate_in,
    normed,
    inv_std,
    norm_gain,
    taps,
    w_proj,
):
    tok_rows, model_width = hidden_state.shape
    top_k = routes.shape[1]
    sp_ways = lax.axis_size("sp")
    tp_parts = lax.axis_size("tp")
    experts = sp_ways // GROUP
    capacity = 3 * tok_rows * top_k // (2 * experts)
    quarter = model_width // tp_parts
    offset = lax.axis_index("tp") * quarter
    slot_place, row_table, row_scale = slot_table(routes, route_weights, experts, capacity)
    zero_row = jnp.zeros((1, model_width), jnp.bfloat16)
    states = jnp.concatenate([hidden_state, zero_row], axis=0)
    cot_pad = jnp.concatenate([out_grad, zero_row], axis=0)
    part_states = lax.dynamic_slice_in_dim(states, offset, quarter, 1)
    part_cots = lax.dynamic_slice_in_dim(cot_pad, offset, quarter, 1)
    sent_rows, sent_cots = pack_rows(
        part_states, part_cots, row_table, row_scale, experts, capacity
    )
    got_rows, got_cots = (
        lax.all_to_all(sent_rows, "sp", split_axis=0, concat_axis=0, tiled=True),
        lax.all_to_all(sent_cots, "sp", split_axis=0, concat_axis=0, tiled=True),
    )
    in_rows, in_cots = (
        lax.all_gather(got_rows, "tp", axis=1, tiled=True),
        lax.all_gather(got_cots, "tp", axis=1, tiled=True),
    )
    gate_wgrad, up_wgrad, down_grad, row_grad = expert_backward(
        in_rows, in_cots, w_gate[0], w_up[0], w_down[0]
    )
    part_sum = lax.psum_scatter(row_grad, "tp", scatter_dimension=1, tiled=True)
    back_rows = lax.all_to_all(part_sum, "sp", split_axis=0, concat_axis=0, tiled=True)
    back_rows = jnp.sum(back_rows.reshape(experts, GROUP, capacity, quarter), axis=1).reshape(
        experts * capacity, quarter
    )
    moe_part = jnp.sum(
        jnp.take(back_rows, slot_place, axis=0).reshape(tok_rows, top_k, quarter), axis=1
    )
    cot_part = lax.dynamic_slice_in_dim(out_grad, offset, quarter, 1)
    stream_part = (cot_part.astype(jnp.float32) + moe_part).astype(jnp.bfloat16)
    stream_full = lax.all_gather(stream_part, "tp", axis=1, tiled=True)
    proj_in = jnp.dot(stream_full, w_proj, preferred_element_type=jnp.float32)
    saved_norm = normed.astype(jnp.float32)
    pre_act = saved_norm * norm_gain[None, :]
    act_sig = jax.nn.sigmoid(pre_act)
    silu_grad = proj_in * act_sig * (1.0 + pre_act * (1.0 - act_sig))
    norm_grad = silu_grad * norm_gain[None, :]
    sum_one, sum_two = lax.psum(
        (jnp.sum(norm_grad, axis=1), jnp.sum(norm_grad * saved_norm, axis=1)), "tp"
    )
    mean_one = sum_one / D_CH
    mean_two = sum_two / D_CH
    conv_grad = inv_std[:, None] * (norm_grad - mean_one[:, None] - saved_norm * mean_two[:, None])
    tail_rows = passed_along(conv_grad[: KSIZE - 1], "sp", -1)
    extended = jnp.concatenate([conv_grad, tail_rows], axis=0)
    glu_grad = taps[0][None, :] * extended[0:tok_rows]
    for tap_index in range(1, KSIZE):
        glu_grad = glu_grad + taps[tap_index][None, :] * extended[tap_index : tap_index + tok_rows]
    input_sig = jax.nn.sigmoid(gate_in.astype(jnp.float32))
    value_grad = (glu_grad * input_sig).astype(jnp.bfloat16)
    gate_in_grad = (glu_grad * value.astype(jnp.float32) * input_sig * (1.0 - input_sig)).astype(
        jnp.bfloat16
    )
    proj_act = (pre_act * act_sig).astype(jnp.bfloat16)
    proj_grad = lax.psum_scatter(
        lax.dot_general(
            stream_full, proj_act, (((0,), (0,)), ((), ())), preferred_element_type=jnp.float32
        ),
        "sp",
        scatter_dimension=0,
        tiled=True,
    )
    return (
        gate_wgrad[None],
        up_wgrad[None],
        down_grad[None],
        stream_part,
        proj_grad,
        value_grad,
        gate_in_grad,
    )


def solution(mesh):
    in_specs = (
        P("sp", None),
        P("sp", None),
        P("sp", None),
        P("sp", None),
        P("sp", None, "tp"),
        P("sp", None, "tp"),
        P("sp", "tp", None),
        P("sp", "tp"),
        P("sp", "tp"),
        P("sp", "tp"),
        P("sp"),
        P("tp"),
        P(None, "tp"),
        P(None, "tp"),
    )
    out_specs = (
        P("sp", None, "tp"),
        P("sp", None, "tp"),
        P("sp", "tp", None),
        P("sp", "tp"),
        P("sp", "tp"),
        P("sp", "tp"),
        P("sp", "tp"),
    )
    return jax.shard_map(
        on_device, mesh=mesh, in_specs=in_specs, out_specs=out_specs, check_vma=False
    )
```

profile of v0, /device:TPU:0, one launch (start us, length us, event | category | flops | bytes accessed | tf_op | source)
XLA Modules:
  0.0 295.3 jit_solution(8357140825040098537)
XLA Ops:
  7.2 0.8 broadcast_multiply_fusion
  8.0 0.8 copy.31
  9.4 1.2 reduce-window.6
  11.0 1.4 scatter_custom_fusion
  12.5 1.0 pad_dynamic-slice_fusion
  13.5 2.1 gather_fusion.1
  15.8 27.4 %all_to_all.33 = bf16[8,96,512]{2,1,0:T(8,128)(2,1)} all-to-all(bf16[8,96,512]{2,1,0:T(8,128)(2,1)S(1)} %bitcast.132), channel_id=1, replica_groups=mesh['sp'=8,'tp'=4] {'sp'}, dimensions={0} | all-to-all | bytes 1572864 | tf_op jit(solution)/shard_map/all_to_all | solution.py:120
  43.5 2.1 gather_fusion.2
  45.5 1.4 scatter_custom_fusion.1
  47.2 23.3 %all_to_all.34 = bf16[8,96,512]{2,1,0:T(8,128)(2,1)} all-to-all(bf16[8,96,512]{2,1,0:T(8,128)(2,1)S(1)} %bitcast.133), channel_id=1, replica_groups=mesh['sp'=8,'tp'=4] {'sp'}, dimensions={0} | all-to-all | bytes 1572864 | tf_op jit(solution)/shard_map/all_to_all | solution.py:121
  70.8 3.7 %fusion.5 = f32[768,448]{0,1:T(8,128)S(1)} fusion(bf16[768,2048]{1,0:T(8,128)(2,1)} %all-gather.3.cloned.1.call-done, bf16[1,2048,448]{1,2,0:T(8,128)(2,1)S(1)} %copy-done), kind=kOutput, calls=%fused_computation.14 | convolution fusion | flops 1409286144 | bytes 6356992 | tf_op jit(solution)/shard_map/dot_general | solution.py:18
  74.5 2.7 fusion.8
  77.2 23.7 %all-gather.5.cloned.1.call-done = bf16[768,2048]{1,0:T(8,128)(2,1)} async-done(((bf16[768,512]{1,0:T(8,128)(2,1)}), bf16[768,2048]{1,0:T(8,128)(2,1)}) %all-gather.5.cloned.1.call-update) | async-done | bytes 3145744 | tf_op jit(solution)/shard_map/all_gather | solution.py:125
  100.9 4.8 %multiply_convert_fusion.1 = (bf16[768,448]{0,1:T(8,128)(2,1)S(1)}, bf16[768,448]{0,1:T(8,128)(2,1)S(1)}) fusion(f32[768,448]{0,1:T(8,128)S(1)} %fusion.5, f32[768,448]{0,1:T(8,128)} %fusion.8, bf16[768,2048]{1,0:T(8,128)(2,1)} %all-gather.5.cloned.1.call-done, bf16[1,448,2048]{2,1,0:T(8,128)(2,1)} %param.22), kind=kOutput, calls=%fused_computation.23 | convolution fusion | flops 1413758976 | bytes 9109504 | tf_op jit(solution)/shard_map/dot_general | solution.py:23
  105.8 1.9 fusion.3
  107.7 4.6 %convolution_add_fusion = f32[768,2048]{1,0:T(8,128)} fusion(f32[768,2048]{1,0:T(8,128)S(1)} %fusion.3, bf16[768,448]{0,1:T(8,128)(2,1)S(1)} %get-tuple-element.14, bf16[1,2048,448]{1,2,0:T(8,128)(2,1)S(1)} %copy-done.2), kind=kOutput, calls=%fused_computation.5 | convolution fusion | flops 1410859008 | bytes 15106048 | tf_op jit(solution)/shard_map/dot_general | solution.py:42
  112.4 58.0 %reduce-scatter.3.cloned.1.call-done = f32[768,512]{1,0:T(8,128)} async-done(((f32[768,2048]{1,0:T(8,128)}), f32[768,512]{1,0:T(8,128)}) %reduce-scatter.3.cloned.1.call-update) | async-done | bytes 1572880 | tf_op jit(solution)/shard_map/reduce_scatter | solution.py:130
  170.4 5.5 %all-to-all-start.2 = ((f32[8,96,512]{2,1,0:T(8,128)}), f32[8,96,512]{2,1,0:T(8,128)}, u32[]{:S(2)}, u32[]{:S(2)}) async-start(f32[8,96,512]{2,1,0:T(8,128)} %bitcast.134), calls=%async_computation.3 | async-start | bytes 3145728 | tf_op jit(solution)/shard_map/all_to_all | solution.py:131
  176.4 5.2 %fusion = bf16[1,448,2048]{2,1,0:T(8,128)(2,1)} fusion(bf16[768,2048]{1,0:T(8,128)(2,1)} %all-gather.5.cloned.1.call-done, f32[768,448]{0,1:T(8,128)} %fusion.8, f32[768,448]{0,1:T(8,128)S(1)} %fusion.5), kind=kOutput, calls=%fused_computation.9 | convolution fusion | flops 1412268032 | bytes 7733248 | tf_op jit(solution)/shard_map/dot_general | solution.py:30
  181.6 31.3 %all-to-all-done.2 = f32[8,96,512]{2,1,0:T(8,128)} async-done(((f32[8,96,512]{2,1,0:T(8,128)}), f32[8,96,512]{2,1,0:T(8,128)}, u32[]{:S(2)}, u32[]{:S(2)}) %all-to-all-start.2) | async-done | bytes 1572896 | tf_op jit(solution)/shard_map/all_to_all | solution.py:131
  212.8 1.6 bitcast_reduce_fusion
  214.5 1.0 gather_fusion
  215.8 0.7 select_reduce_fusion
  216.5 1.0 add_convert_fusion
  217.6 6.7 %all_gather.11 = bf16[128,2048]{1,0:T(8,128)(2,1)S(1)} all-gather(bf16[128,512]{1,0:T(8,128)(2,1)S(1)} %add_convert_fusion), channel_id=1, replica_groups=mesh['sp'=8,'tp'=4] {'tp'}, dimensions={1}, use_global_device_ids=true | all-gather | bytes 655360 | tf_op jit(solution)/shard_map/all_gather | solution.py:140
  224.3 1.3 fusion.116
  225.7 4.8 %fusion.2 = bf16[1,2048,448]{1,2,0:T(8,128)(2,1)} fusion(bf16[768,448]{0,1:T(8,128)(2,1)S(1)} %copy-done.4, bf16[768,2048]{1,0:T(8,128)(2,1)} %all-gather.3.cloned.1.call-done), kind=kOutput, calls=%fused_computation.11 | convolution fusion | flops 1410203648 | bytes 5668864 | tf_op jit(solution)/shard_map/dot_general | solution.py:36
  230.8 7.2 %all-reduce.2 = (f32[128]{0:T(128)S(1)}, f32[128]{0:T(128)S(1)}) all-reduce(f32[128]{0:T(128)S(1)} %get-tuple-element.9, f32[128]{0:T(128)S(1)} %get-tuple-element.8), channel_id=1, replica_groups=mesh['sp'=8,'tp'=4] {'tp'}, use_global_device_ids=true, to_apply=%region_12.14 | all-reduce | flops 256 | bytes 2048 | tf_op jit(solution)/shard_map/psum | solution.py:147
  238.2 1.3 collective-permute-start
  239.5 5.0 %fusion.1 = bf16[1,2048,448]{1,2,0:T(8,128)(2,1)} fusion(bf16[768,448]{0,1:T(8,128)(2,1)} %copy-done.16, bf16[768,2048]{1,0:T(8,128)(2,1)} %all-gather.3.cloned.1.call-done), kind=kOutput, calls=%fused_computation.10 | convolution fusion | flops 1410203648 | bytes 5668864 | tf_op jit(solution)/shard_map/dot_general | solution.py:33
  244.5 0.9 multiply_convert_fusion.5
  246.0 42.7 %reduce-scatter.5.cloned.1.call-done = f32[256,128]{1,0:T(8,128)} async-done(((f32[2048,128]{1,0:T(8,128)}), f32[256,128]{1,0:T(8,128)}) %reduce-scatter.5.cloned.1.call-update) | async-done | bytes 131088 | tf_op jit(solution)/shard_map/reduce_scatter | solution.py:164
  (81 shorter events, 4.2 us)
Async XLA Ops:
  7.2 63.7 %copy-start = (bf16[1,2048,448]{1,2,0:T(8,128)(2,1)S(1)}, bf16[1,2048,448]{1,2,0:T(8,128)(2,1)}, u32[]{:S(2)}) copy-start(bf16[1,2048,448]{1,2,0:T(8,128)(2,1)} %param.20) | copy-start | bytes 5505028
  7.2 63.6 %all-gather.3.cloned.1.call-start = ((), (), s32[]{:S(2)}) async-start(), calls=%async_computation.5 | async-start | bytes 3932160 | tf_op jit(solution)/shard_map/all_gather | solution.py:124
  15.7 27.5 %copy-start.11 = (f32[128,2]{0,1:T(2,128)S(1)}, f32[128,2]{0,1:T(2,128)}, u32[]{:S(2)}) copy-start(f32[128,2]{0,1:T(2,128)} %param.19) | copy-start | bytes 3076
  43.1 57.8 %all-gather.5.cloned.1.call-start = ((), (), s32[]{:S(2)}) async-start(), calls=%async_computation.6 | async-start | bytes 3932160 | tf_op jit(solution)/shard_map/all_gather | solution.py:125
  70.5 99.9 %reduce-scatter.3.cloned.1.call-start = ((), (), s32[]{:S(2)}) async-start(), calls=%async_computation.7 | async-start | bytes 7864320 | tf_op jit(solution)/shard_map/reduce_scatter | solution.py:130
  70.8 3.7 %copy-start.1 = (bf16[1,2048,448]{1,2,0:T(8,128)(2,1)S(1)}, bf16[1,2048,448]{1,2,0:T(8,128)(2,1)}, u32[]{:S(2)}) copy-start(bf16[1,2048,448]{1,2,0:T(8,128)(2,1)} %param.21) | copy-start | bytes 5505028
  70.8 3.7 %copy-start.14 = (bf16[768,2048]{1,0:T(8,128)(2,1)S(1)}, bf16[768,2048]{1,0:T(8,128)(2,1)}, u32[]{:S(2)}) copy-start(bf16[768,2048]{1,0:T(8,128)(2,1)} %all-gather.3.cloned.1.call-done) | copy-start | bytes 9437188
  105.7 1.9 copy-start.16
  105.7 1.9 copy-start.3
  105.7 2.0 copy-start.2
  112.4 63.8 %copy-start.10 = (s32[128,2]{0,1:T(2,128)S(1)}, s32[128,2]{0,1:T(2,128)}, u32[]{:S(2)}) copy-start(s32[128,2]{0,1:T(2,128)} %param.18) | copy-start | bytes 3076
  112.4 64.0 %copy-start.9 = (f32[31,128]{1,0:T(8,128)S(1)}, f32[31,128]{1,0:T(8,128)}, u32[]{:S(2)}) copy-start(f32[31,128]{1,0:T(8,128)} %param.28) | copy-start | bytes 47620
  170.4 42.4 %all-to-all-start.2 = ((f32[8,96,512]{2,1,0:T(8,128)}), f32[8,96,512]{2,1,0:T(8,128)}, u32[]{:S(2)}, u32[]{:S(2)}) async-start(f32[8,96,512]{2,1,0:T(8,128)} %bitcast.134), calls=%async_computation.3 | async-start | bytes 3145728 | tf_op jit(solution)/shard_map/all_to_all | solution.py:131
  175.9 112.8 %reduce-scatter.5.cloned.1.call-start = ((), (), s32[]{:S(2)}) async-start(), calls=%async_computation.8 | async-start | bytes 1179648 | tf_op jit(solution)/shard_map/reduce_scatter | solution.py:164
  215.4 8.8 %copy-start.6 = (bf16[128,128]{1,0:T(8,128)(2,1)S(1)}, bf16[128,128]{1,0:T(8,128)(2,1)}, u32[]{:S(2)}) copy-start(bf16[128,128]{1,0:T(8,128)(2,1)} %param.25) | copy-start | bytes 98308
  215.5 8.8 %copy-start.12 = (f32[128]{0:T(128)S(1)}, f32[128]{0:T(128)}, u32[]{:S(2)}) copy-start(f32[128]{0:T(128)} %param.27) | copy-start | bytes 1540
  216.5 9.1 %copy-start.4 = (bf16[768,448]{0,1:T(8,128)(2,1)S(1)}, bf16[768,448]{0,1:T(8,128)(2,1)}, u32[]{:S(2)}) copy-start(bf16[768,448]{0,1:T(8,128)(2,1)} %copy-done.3) | copy-start | bytes 2064388
  217.6 12.9 %copy-start.5 = (bf16[128,512]{1,0:T(8,128)(2,1)}, bf16[128,512]{1,0:T(8,128)(2,1)S(1)}, u32[]{:S(2)}) copy-start(bf16[128,512]{1,0:T(8,128)(2,1)S(1)} %add_convert_fusion) | copy-start | bytes 393220
  225.6 4.8 %copy-start.15 = (bf16[2048,128]{1,0:T(8,128)(2,1)S(1)}, bf16[2048,128]{1,0:T(8,128)(2,1)}, u32[]{:S(2)}) copy-start(bf16[2048,128]{1,0:T(8,128)(2,1)} %param.29) | copy-start | bytes 1572868
  225.7 12.4 %copy-start.13 = (f32[128]{0:T(128)S(1)}, f32[128]{0:T(128)}, u32[]{:S(2)}) copy-start(f32[128]{0:T(128)} %param.26) | copy-start | bytes 1540
  238.2 6.3 %copy-start.7 = (bf16[128,128]{1,0:T(8,128)(2,1)S(1)}, bf16[128,128]{1,0:T(8,128)(2,1)}, u32[]{:S(2)}) copy-start(bf16[128,128]{1,0:T(8,128)(2,1)} %param.24) | copy-start | bytes 98308
  238.2 6.3 %copy-start.8 = (bf16[128,128]{1,0:T(8,128)(2,1)S(1)}, bf16[128,128]{1,0:T(8,128)(2,1)}, u32[]{:S(2)}) copy-start(bf16[128,128]{1,0:T(8,128)(2,1)} %param.23) | copy-start | bytes 98308
  238.2 6.3 %collective-permute-start = (f32[30,128]{1,0:T(8,128)S(1)}, f32[30,128]{1,0:T(8,128)S(1)}, u32[]{:S(2)}, u32[]{:S(2)}) collective-permute-start(f32[30,128]{1,0:T(8,128)S(1)} %slice.263), channel_id=1, source_target_pairs={{4,0},{8,4},{12,8},{16,12},{20,16},{24,20},{28,24},{5,1},{9,5},{13... | collective-permute-start | bytes 46088 | tf_op jit(solution)/shard_map/ppermute | solution.py:14
Sparse Core Ops, SparseCore 0:
  43.3 27.5 all-gather.2
  72.4 28.4 all-gather.4
  112.5 57.8 reduce-scatter.2
  225.8 62.9 reduce-scatter.4
where the time goes:
time: 296 us; the launch traced here: 295 us
  waiting for transfers between devices  156 us (53%)
  blocking collectives  64.6 us (22%)
  matrix products  34.3 us (12%)
  between operations  14.2 us (5%)
  local copies, waits for them, and re-layouts  11.7 us (4%)
  other arithmetic  7.55 us (3%)
  starting transfers between devices  7.15 us (2%)
    reduce_scatter x1, waiting for transfers between devices, on_device(): part_sum = lax.psum_scatter(row_grad, 'tp', scatter_dimension=1, tiled=True)  58 us
    reduce_scatter x1, waiting for transfers between devices, on_device(): lax.psum_scatter(lax.dot_general(stream_full, proj_act, (((0,), (0,)), ((...  42.7 us
    all_to_all x1, waiting for transfers between devices, on_device(): lax.all_to_all(part_sum, 'sp', split_axis=0, concat_axis=0, tiled=True)  31.3 us
    all_to_all x1, blocking collectives, on_device(): lax.all_to_all(sent_rows, 'sp', split_axis=0, concat_axis=0, tiled=True)  27.4 us
    all_gather x1, waiting for transfers between devices, on_device(): lax.all_gather(got_cots, 'tp', axis=1, tiled=True)  23.7 us
    all_to_all x1, blocking collectives, on_device(): lax.all_to_all(sent_cots, 'sp', split_axis=0, concat_axis=0, tiled=True)  23.3 us
    psum x1, blocking collectives, on_device(): lax.psum((jnp.sum(norm_grad, axis=1), jnp.sum(norm_grad * saved_norm, axi...  7.21 us
    all_gather x1, blocking collectives, on_device(): stream_full = lax.all_gather(stream_part, 'tp', axis=1, tiled=True)  6.72 us
  transfers between devices with their start and end apart: 6, of which 5 were waited for; matrix products, arithmetic and copies ran while one was open for 9% of the time, Pallas kernels for 0%

commit v1 on v0

v1 whole, which is shorter than its diff:
```python
import functools

import jax
import jax.numpy as jnp
from jax import lax
from jax.experimental import pallas as pl
from jax.experimental.pallas import tpu as pltpu
from jax.sharding import PartitionSpec as P

GROUP = 2
PAIR = 2
MESH = pl.DeviceIdType.MESH
F32 = jnp.float32
BF16 = jnp.bfloat16


def dot_rows(a, b):
    return lax.dot_general(a, b, (((0,), (0,)), ((), ())), preferred_element_type=F32)


def dot_cols(a, b):
    return lax.dot_general(a, b, (((1,), (1,)), ((), ())), preferred_element_type=F32)


def place():
    s, t = lax.axis_index("sp"), lax.axis_index("tp")
    e, g = s // GROUP, s % GROUP
    hi, lo = t // PAIR, t % PAIR
    across = (s, (1 - hi) * PAIR + lo)
    beside = (e * GROUP + 1 - g, t)
    partner = (s, hi * PAIR + 1 - lo)
    return s, t, e, g, hi, lo, across, beside, partner


def greet(devices):
    barrier = pltpu.get_barrier_semaphore()
    for device in devices:
        pl.semaphore_signal(barrier, inc=1, device_id=device, device_id_type=MESH)
    pl.semaphore_wait(barrier, len(devices))


def remote(src, dst, send, recv, device):
    return pltpu.make_async_remote_copy(
        src_ref=src, dst_ref=dst, send_sem=send, recv_sem=recv, device_id=device, device_id_type=MESH
    )


def one_hot(rank_row, cap):
    slots = lax.broadcasted_iota(jnp.int32, (cap, rank_row.shape[1]), 0)
    return jnp.where(slots == rank_row, 1.0, 0.0)


def dispatch_kernel(experts, cap, h_ref, c_ref, rank_ref, w_ref, out_ref, pack, z_send, z_recv, g_send, g_recv):
    s, t, e, g, hi, lo, across, beside, partner = place()
    quarter = h_ref.shape[1]
    across_t = across[1]

    def loc(j, side, col):
        src = lax.rem(e + experts - j, experts)
        rows = pl.ds(pl.multiple_of((src * GROUP + side) * cap, cap), cap)
        cols = pl.ds(pl.multiple_of(col * quarter, quarter), quarter)
        return rows, cols

    z_peers = [(lax.rem(e + j, experts) * GROUP + g, t) for j in range(1, experts)]
    greet(z_peers + [across, beside, partner])
    sent = []
    own_rows, own_cols = loc(0, g, t)
    for j in list(range(1, experts)) + [0]:
        target = lax.rem(e + j, experts)
        rank_row = rank_ref[pl.ds(target, 1), :]
        hot = one_hot(rank_row, cap)
        scale = jnp.sum(hot * w_ref[pl.ds(target, 1), :], axis=1, keepdims=True)
        hot = hot.astype(BF16)
        rows = jnp.dot(hot, h_ref[...], preferred_element_type=F32).astype(BF16)
        cots = (jnp.dot(hot, c_ref[...], preferred_element_type=F32) * scale).astype(BF16)
        if j:
            pack[j, 0] = rows
            pack[j, 1] = cots
            copy = remote(
                pack.at[j], out_ref.at[:, own_rows, own_cols], z_send.at[j], z_recv.at[j], z_peers[j - 1]
            )
            copy.start()
            sent.append(copy)
        else:
            out_ref[0, own_rows, own_cols] = rows
            out_ref[1, own_rows, own_cols] = cots

    def hop(n, j, ref, device):
        return remote(ref, ref, g_send.at[j, n], g_recv.at[j, n], device)

    def send(n, j, ref, device):
        copy = hop(n, j, ref, device)
        copy.start()
        sent.append(copy)

    def full(j, side, col):
        rows, cols = loc(j, side, col)
        return out_ref.at[:, rows, cols]

    def part(k, j, side, col):
        rows, cols = loc(j, side, col)
        return out_ref.at[k, rows, cols]

    def arrived(n, j, ref):
        hop(n, j, ref, partner).wait_recv()

    def first(j):
        if j:
            block = full(j, g, t)
            remote(block, block, z_send.at[j], z_recv.at[j], partner).wait_recv()
        block = full(j, g, t)
        send(0, j, block, across)
        send(1, j, block, beside)
        send(2, j, block, partner)

    def second(j):
        arrived(0, j, full(j, g, across_t))
        send(3, j, part(0, j, g, across_t), beside)
        send(5, j, full(j, g, across_t), partner)
        arrived(1, j, full(j, 1 - g, t))
        send(4, j, part(1, j, 1 - g, t), across)
        send(6, j, full(j, 1 - g, t), partner)

    def third(j):
        arrived(3, j, part(0, j, 1 - g, across_t))
        send(7, j, part(0, j, 1 - g, across_t), partner)
        arrived(4, j, part(1, j, 1 - g, across_t))
        send(8, j, part(1, j, 1 - g, across_t), partner)

    for j in range(experts + 2):
        if j < experts:
            first(j)
        if 0 <= j - 1 < experts:
            second(j - 1)
        if 0 <= j - 2:
            third(j - 2)
    other_t = partner[1]
    far_t = (1 - hi) * PAIR + 1 - lo
    for j in range(experts):
        arrived(2, j, full(j, g, other_t))
        arrived(5, j, full(j, g, far_t))
        arrived(6, j, full(j, 1 - g, other_t))
        arrived(7, j, part(0, j, 1 - g, far_t))
        arrived(8, j, part(1, j, 1 - g, far_t))
    for copy in sent:
        copy.wait_send()


def dispatch(h_part, c_part, rank, weight, experts, cap, rows, width):
    vmem = pl.BlockSpec(memory_space=pltpu.VMEM)
    quarter = h_part.shape[1]
    return pl.pallas_call(
        functools.partial(dispatch_kernel, experts, cap),
        out_shape=jax.ShapeDtypeStruct((2, rows, width), BF16),
        in_specs=[vmem] * 4,
        out_specs=vmem,
        scratch_shapes=[
            pltpu.VMEM((experts, 2, cap, quarter), BF16),
            pltpu.SemaphoreType.DMA((experts,)),
            pltpu.SemaphoreType.DMA((experts,)),
            pltpu.SemaphoreType.DMA((experts, 9)),
            pltpu.SemaphoreType.DMA((experts, 9)),
        ],
        compiler_params=pltpu.CompilerParams(
            collective_id=0, has_side_effects=True, vmem_limit_bytes=40 * 1024 * 1024
        ),
        name="dispatch",
    )(h_part, c_part, rank, weight)


def tail_kernel(
    experts, cap, ksize,
    grad_ref, rank_ref, cot_ref, value_ref, gate_ref, normed_ref, std_ref, gain_ref, taps_ref, proj_ref,
    stream_ref, pgrad_ref, vgrad_ref, ggrad_ref,
    from_core, sums, rx_a, ry_b, relay, rx2, back, done, full, stats, ext, pg, py, pz_out, pz,
    core_send, core_recv, hop_send, hop_recv, z_send, z_recv, t_send, t_recv, p_send, p_recv, q_send, q_recv,
):
    s, t, e, g, hi, lo, across, beside, partner = place()
    sp_ways = experts * GROUP
    tok, quarter = cot_ref.shape
    half = quarter // 2
    tp_ways = stats.shape[0]
    z_peers = [(lax.rem(e + j, experts) * GROUP + g, t) for j in range(1, experts)]
    far = (s, (1 - hi) * PAIR + 1 - lo)
    before = (lax.rem(s + sp_ways - 1, sp_ways), t)
    after = (lax.rem(s + 1, sp_ways), t)
    greet(z_peers + [across, beside, partner, far, before, after])
    sent = []

    def go(copy):
        copy.start()
        sent.append(copy)

    order = list(range(1, experts)) + [0]

    def rows_of(j):
        target = lax.rem(e + j, experts)
        return pl.ds(pl.multiple_of(target * GROUP * cap, cap), GROUP * cap)

    def cols_of(col):
        return pl.ds(pl.multiple_of(col * quarter, quarter), quarter)

    def core_copy(j, h, lane):
        return remote(
            grad_ref.at[rows_of(j), cols_of(h * PAIR + lane)],
            from_core.at[j, h],
            core_send.at[j, h],
            core_recv.at[j, h],
            partner,
        )

    for j in order:
        for h in range(PAIR):
            go(core_copy(j, h, 1 - lo))

    def hop_copy(n, j, src, dst, device):
        return remote(src, dst, hop_send.at[j, n], hop_recv.at[j, n], device)

    def x_first(j):
        return hop_copy(0, j, sums.at[0, j, 1 - hi], rx_a.at[j], across)

    def y_first(j):
        return hop_copy(1, j, sums.at[1, j, :, 1 - g], ry_b.at[j], beside)

    def y_second(j):
        return hop_copy(2, j, relay.at[0, j], rx2.at[0, j], beside)

    def x_second(j):
        return hop_copy(3, j, relay.at[1, j], rx2.at[1, j], across)

    def z_copy(j):
        return remote(done.at[j], back.at[j], z_send.at[j], z_recv.at[j], z_peers[j - 1])

    def first(j):
        for h in range(PAIR):
            core_copy(j, h, lo).wait_recv()
            mine = grad_ref[rows_of(j), cols_of(h * PAIR + lo)].astype(F32)
            total = (mine + from_core[j, h].astype(F32)).astype(BF16).reshape(GROUP, cap, quarter)
            sums[0, j, h] = total[:, :, :half]
            sums[1, j, h] = total[:, :, half:]
        go(x_first(j))
        go(y_first(j))

    def second(j):
        x_first(j).wait_recv()
        relay[0, j] = (sums[0, j, hi, 1 - g].astype(F32) + rx_a[j, 1 - g].astype(F32)).astype(BF16)
        go(y_second(j))
        y_first(j).wait_recv()
        relay[1, j] = (sums[1, j, 1 - hi, g].astype(F32) + ry_b[j, 1 - hi].astype(F32)).astype(BF16)
        go(x_second(j))

    def third(j):
        y_second(j).wait_recv()
        done[j, :, :half] = (
            sums[0, j, hi, g].astype(F32) + rx_a[j, g].astype(F32) + rx2[0, j].astype(F32)
        ).astype(BF16)
        x_second(j).wait_recv()
        done[j, :, half:] = (
            sums[1, j, hi, g].astype(F32) + ry_b[j, hi].astype(F32) + rx2[1, j].astype(F32)
        ).astype(BF16)
        if j:
            go(z_copy(j))

    for i in range(experts + 2):
        if i < experts:
            first(order[i])
        if 0 <= i - 1 < experts:
            second(order[i - 1])
        if 0 <= i - 2:
            third(order[i - 2])

    gain = gain_ref[...]
    saved = normed_ref[...].astype(F32)
    pre_act = saved * gain
    act_sig = jax.nn.sigmoid(pre_act)
    slope = act_sig * (1.0 + pre_act * (1.0 - act_sig))
    proj_act = (pre_act * act_sig).astype(BF16)

    stream = cot_ref[...].astype(F32)
    for j in [0] + list(range(1, experts)):
        if j:
            z_copy(j).wait_recv()
            block = back[j]
        else:
            block = done[0]
        source = lax.rem(e + experts - j, experts)
        hot = one_hot(rank_ref[pl.ds(source, 1), :], cap).astype(BF16)
        stream = stream + dot_rows(hot, block)
    stream = stream.astype(BF16)
    stream_ref[...] = stream
    full[:, cols_of(t)] = stream

    def gather_copy(n, col, device):
        return remote(full.at[:, cols_of(col)], full.at[:, cols_of(col)], t_send.at[n], t_recv.at[n], device)

    go(gather_copy(0, t, across))
    go(gather_copy(1, t, partner))
    gather_copy(0, across[1], across).wait_recv()
    go(gather_copy(2, across[1], partner))
    gather_copy(1, partner[1], partner).wait_recv()
    gather_copy(2, far[1], partner).wait_recv()

    rows = pg.shape[2]

    def p_copy(j):
        return remote(pg.at[j, 1 - g], py.at[j], p_send.at[j], p_recv.at[j], beside)

    whole = dot_rows(full[...], proj_act)
    pall = whole.reshape(experts, GROUP, rows, whole.shape[1])
    for i in range(experts):
        pg[i] = pall[i].astype(BF16)
    for i in range(experts):
        go(p_copy(i))

    proj_in = jnp.dot(full[...], proj_ref[...], preferred_element_type=F32)
    norm_grad = proj_in * slope * gain
    one = jnp.sum(norm_grad, axis=1, keepdims=True)
    two = jnp.sum(norm_grad * saved, axis=1, keepdims=True)
    lane = lax.broadcasted_iota(jnp.int32, (tok, 128), 1)
    packed = jnp.where(lane == 0, one, jnp.where(lane == 1, two, 0.0))
    stats[t] = packed.T[:8]

    def stat_copy(n, device, owner):
        return remote(stats.at[owner], stats.at[owner], t_send.at[n], t_recv.at[n], device)

    for n, device in ((3, across), (4, far), (5, partner)):
        go(stat_copy(n, device, t))

    def q_copy(j):
        return remote(pz_out.at[j], pz.at[j], q_send.at[j], q_recv.at[j], z_peers[j - 1])

    for n, device in ((3, across), (4, far), (5, partner)):
        stat_copy(n, device, device[1]).wait_recv()
    total = stats[0]
    for i in range(1, tp_ways):
        total = total + stats[i]
    total = jnp.concatenate([total, jnp.zeros((120, tok), F32)], axis=0).T
    channels = saved.shape[1] * tp_ways
    mean_one = total[:, 0:1] / channels
    mean_two = total[:, 1:2] / channels
    conv = std_ref[...] * (norm_grad - mean_one - saved * mean_two)
    ext[pl.ds(0, tok), :] = conv

    def halo_copy():
        return remote(ext.at[pl.ds(0, 32)], ext.at[pl.ds(tok, 32)], t_send.at[6], t_recv.at[6], before)

    @pl.when(s > 0)
    def _():
        halo_copy().start()

    for i in range(experts):
        p_copy(i).wait_recv()
    for j in order:
        target = lax.rem(e + j, experts)
        piece = pg[target, g].astype(F32) + py[target].astype(F32)
        if j:
            pz_out[j] = piece.astype(BF16)
            go(q_copy(j))
        else:
            pgrad_ref[...] = piece

    @pl.when(s < sp_ways - 1)
    def _():
        halo_copy().wait_recv()

    @pl.when(s == sp_ways - 1)
    def _():
        ext[pl.ds(tok, 32), :] = jnp.zeros((32, ext.shape[1]), F32)

    glu = taps_ref[0:1, :] * ext[pl.ds(0, tok), :]
    for k in range(1, ksize):
        glu = glu + taps_ref[k : k + 1, :] * ext[pl.ds(k, tok), :]
    in_sig = jax.nn.sigmoid(gate_ref[...].astype(F32))
    vgrad_ref[...] = (glu * in_sig).astype(BF16)
    ggrad_ref[...] = (glu * value_ref[...].astype(F32) * in_sig * (1.0 - in_sig)).astype(BF16)

    total = pgrad_ref[...]
    for j in range(1, experts):
        q_copy(j).wait_recv()
        total = total + pz[j].astype(F32)
    pgrad_ref[...] = total

    @pl.when(s > 0)
    def _():
        halo_copy().wait_send()

    for copy in sent:
        copy.wait_send()


def tail(grad, rank, cot, value, gate_in, normed, std, gain, taps, w_proj, experts, cap, tp_ways):
    vmem = pl.BlockSpec(memory_space=pltpu.VMEM)
    tok, quarter = cot.shape
    width = grad.shape[1]
    ch = normed.shape[1]
    rows = width // (experts * GROUP)
    half = quarter // 2
    dma = pltpu.SemaphoreType.DMA
    assert ksize_ok(taps.shape[0])
    return pl.pallas_call(
        functools.partial(tail_kernel, experts, cap, taps.shape[0]),
        out_shape=(
            jax.ShapeDtypeStruct((tok, quarter), BF16),
            jax.ShapeDtypeStruct((rows, ch), F32),
            jax.ShapeDtypeStruct((tok, ch), BF16),
            jax.ShapeDtypeStruct((tok, ch), BF16),
        ),
        in_specs=[vmem] * 10,
        out_specs=(vmem,) * 4,
        scratch_shapes=[
            pltpu.VMEM((experts, PAIR, GROUP * cap, quarter), BF16),
            pltpu.VMEM((2, experts, PAIR, GROUP, cap, half), BF16),
            pltpu.VMEM((experts, GROUP, cap, half), BF16),
            pltpu.VMEM((experts, PAIR, cap, half), BF16),
            pltpu.VMEM((2, experts, cap, half), BF16),
            pltpu.VMEM((2, experts, cap, half), BF16),
            pltpu.VMEM((experts, cap, quarter), BF16),
            pltpu.VMEM((experts, cap, quarter), BF16),
            pltpu.VMEM((tok, width), BF16),
            pltpu.VMEM((tp_ways, 8, tok), F32),
            pltpu.VMEM((tok + 32, ch), F32),
            pltpu.VMEM((experts, GROUP, rows, ch), BF16),
            pltpu.VMEM((experts, rows, ch), BF16),
            pltpu.VMEM((experts, rows, ch), BF16),
            pltpu.VMEM((experts, rows, ch), BF16),
            dma((experts, PAIR)),
            dma((experts, PAIR)),
            dma((experts, 4)),
            dma((experts, 4)),
            dma((experts,)),
            dma((experts,)),
            dma((7,)),
            dma((7,)),
            dma((experts,)),
            dma((experts,)),
            dma((experts,)),
            dma((experts,)),
        ],
        compiler_params=pltpu.CompilerParams(
            collective_id=1, has_side_effects=True, vmem_limit_bytes=56 * 1024 * 1024
        ),
        name="tail",
    )(grad, rank, cot, value, gate_in, normed, std, gain, taps, w_proj)


def ksize_ok(taps):
    return taps - 1 <= 32


def expert_backward(in_rows, in_cots, gate_slice, up_slice, down_slice):
    pre_gate = jnp.dot(in_rows, gate_slice, preferred_element_type=F32)
    pre_up = jnp.dot(in_rows, up_slice, preferred_element_type=F32)
    gate_sig = jax.nn.sigmoid(pre_gate)
    silu_gate = pre_gate * gate_sig
    act_rows = (silu_gate * pre_up).astype(BF16)
    act_grad = dot_cols(in_cots, down_slice)
    gate_grad = (act_grad * pre_up * gate_sig * (1.0 + pre_gate * (1.0 - gate_sig))).astype(BF16)
    up_grad = (act_grad * silu_gate).astype(BF16)
    row_grad = (dot_cols(gate_grad, gate_slice) + dot_cols(up_grad, up_slice)).astype(BF16)
    down_grad = dot_rows(act_rows, in_cots).astype(BF16)
    gate_wgrad = dot_rows(in_rows, gate_grad).astype(BF16)
    up_wgrad = dot_rows(in_rows, up_grad).astype(BF16)
    return gate_wgrad, up_wgrad, down_grad, row_grad


def on_device(
    hidden_state, out_grad, routes, route_weights, w_gate, w_up, w_down,
    value, gate_in, normed, inv_std, norm_gain, taps, w_proj,
):
    tok, width = hidden_state.shape
    top_k = routes.shape[1]
    sp_ways, tp_ways = lax.axis_size("sp"), lax.axis_size("tp")
    experts = sp_ways // GROUP
    cap = 3 * tok * top_k // (2 * experts)
    cap = -(-cap // 16) * 16
    quarter = width // tp_ways
    offset = lax.axis_index("tp") * quarter
    names = routes[None, :, :] == jnp.arange(experts, dtype=jnp.int32)[:, None, None]
    named = jnp.any(names, axis=2)
    weight = jnp.sum(jnp.where(names, route_weights[None], 0.0), axis=2)
    index = jnp.arange(tok)
    earlier = (index[:, None] < index[None, :]).astype(BF16)
    rank = jnp.dot(named.astype(BF16), earlier, preferred_element_type=F32).astype(jnp.int32)
    rank = jnp.where(named, rank, -1)
    h_part = lax.dynamic_slice_in_dim(hidden_state, offset, quarter, 1)
    c_part = lax.dynamic_slice_in_dim(out_grad, offset, quarter, 1)
    got = dispatch(h_part, c_part, rank, weight, experts, cap, sp_ways * cap, width)
    gate_wgrad, up_wgrad, down_grad, row_grad = expert_backward(got[0], got[1], w_gate[0], w_up[0], w_down[0])
    stream_part, proj_grad, value_grad, gate_in_grad = tail(
        row_grad, rank, c_part, value, gate_in, normed, inv_std[:, None], norm_gain[None, :], taps, w_proj,
        experts, cap, tp_ways,
    )
    return gate_wgrad[None], up_wgrad[None], down_grad[None], stream_part, proj_grad, value_grad, gate_in_grad


def solution(mesh):
    in_specs = (
        P("sp", None), P("sp", None), P("sp", None), P("sp", None),
        P("sp", None, "tp"), P("sp", None, "tp"), P("sp", "tp", None),
        P("sp", "tp"), P("sp", "tp"), P("sp", "tp"), P("sp"), P("tp"), P(None, "tp"), P(None, "tp"),
    )
    out_specs = (
        P("sp", None, "tp"), P("sp", None, "tp"), P("sp", "tp", None),
        P("sp", "tp"), P("sp", "tp"), P("sp", "tp"), P("sp", "tp"),
    )
    return jax.shard_map(on_device, mesh=mesh, in_specs=in_specs, out_specs=out_specs, check_vma=False)
```

time: 296 us -> 117 us (0.40)
  waiting for transfers between devices: 156 us -> 0 us
  Pallas kernels: 0 us -> 86.7 us
  blocking collectives: 64.6 us -> 0 us
  matrix products: 34.3 us -> 19.6 us
  between operations: 14.2 us -> 0.75 us
  starting transfers between devices: 7.15 us -> 0 us
  other arithmetic: 7.55 us -> 1.54 us
  local copies, waits for them, and re-layouts: 11.7 us -> 8.29 us
    reduce_scatter x2 -> x0, waiting for transfers between devices: 101 us -> none  [the longest x1 58 us: on_device(): part_sum = lax.psum_scatter(row_grad, 'tp', scatter_dimension=1, tiled=True)]
    pallas_call x0 -> x2, Pallas kernels: none -> 86.7 us  [the longest x1 47.7 us: tail(): pl.pallas_call(functools.partial(tail_kernel, experts, cap, taps.shape[0]...]
    all_to_all x2 -> x0, blocking collectives: 50.7 us -> none  [the longest x1 27.4 us: on_device(): lax.all_to_all(sent_rows, 'sp', split_axis=0, concat_axis=0, tiled=True)]
    all_to_all x1 -> x0, waiting for transfers between devices: 31.3 us -> none  [on_device(): lax.all_to_all(part_sum, 'sp', split_axis=0, concat_axis=0, tiled=True)]
    all_gather x2 -> x0, waiting for transfers between devices: 23.7 us -> none  [the longest x1 23.7 us: on_device(): lax.all_gather(got_cots, 'tp', axis=1, tiled=True)]
    dot_general x10 -> x9, matrix products: 34.3 us -> 19.6 us  [the longest x3 8.61 us: dot_rows(): lax.dot_general(a, b, (((0,), (0,)), ((), ())), preferred_element_type=F32)]
    psum x1 -> x0, blocking collectives: 7.21 us -> none  [on_device(): lax.psum((jnp.sum(norm_grad, axis=1), jnp.sum(norm_grad * saved_norm, axi...]
    all_gather x1 -> x0, blocking collectives: 6.72 us -> none  [on_device(): stream_full = lax.all_gather(stream_part, 'tp', axis=1, tiled=True)]
  transfers between devices with their start and end apart: 6 -> 0, of which waited for: 5 -> 0; matrix products, arithmetic and copies ran while one was open for 9% -> 0% of each run, Pallas kernels for 0% -> 0%
where the time goes in v1:
time: 117 us
  Pallas kernels  86.7 us (74%)
  matrix products  19.6 us (17%)
  local copies, waits for them, and re-layouts  8.29 us (7%)
  other arithmetic  1.54 us (1%)
    pallas_call x1, Pallas kernels, tail(): pl.pallas_call(functools.partial(tail_kernel, experts, cap, taps.shape[0]...  47.7 us
    pallas_call x1, Pallas kernels, dispatch(): pl.pallas_call(functools.partial(dispatch_kernel, experts, cap), out_shap...  38.9 us
    dot_general x3, matrix products, dot_rows(): lax.dot_general(a, b, (((0,), (0,)), ((), ())), preferred_element_type=F32)  8.61 us
    dot_general x3, matrix products, dot_cols(): lax.dot_general(a, b, (((1,), (1,)), ((), ())), preferred_element_type=F32)  7.55 us
    unnamed x14, local copies, waits for them, and re-layouts  5.91 us

profile of v1, /device:TPU:0, one launch (start us, length us, event | category | flops | bytes accessed | tf_op | source)
XLA Modules:
  0.0 116.8 jit_solution(2159755965242449814)
XLA Ops:
  0.6 0.0 copy-start
  0.7 0.8 fusion.45
  1.5 0.1 fusion.43.rank_ref
  1.6 0.0 copy-start.2
  1.6 0.7 select_reduce_fusion.w_ref
  2.3 1.4 %copy.24.std_ref = f32[128,1]{1,0:T(8,128)} copy(f32[128,1]{0,1:T(1,128)} %bitcast.56) | data formatting | bytes 1024 | tf_op jit(solution)/shard_map/broadcast_in_dim | solution.py:490
  3.7 1.0 constant_dynamic-slice_fusion
  4.7 0.0 copy-start.1
  4.7 38.9 %dispatch.1 = bf16[2,768,2048]{2,1,0:T(8,128)(2,1)S(1)} custom-call(bf16[128,512]{1,0:T(8,128)(2,1)S(1)} %get-tuple-element.18.h_ref, bf16[128,512]{1,0:T(8,128)(2,1)S(1)} %get-tuple-element.17.c_ref.cot_ref, s32[4,128]{1,0:T(4,128)S(1)} %fusion.43.rank_ref, f32[4,128]{1,0:T(4,128)S(1)} %select_reduce_fusion.w_ref), custom_call_target="tpu_custom_call" | custom-call | tf_op jit(solution)/shard_map/dispatch/pallas_call | solution.py:152
  43.7 0.0 copy-done.2
  43.7 0.0 copy-done.1
  43.7 0.0 copy-done
  43.7 0.0 copy-start.4
  43.7 1.6 %fusion.8 = f32[768,448]{0,1:T(8,128)S(1)} fusion(bf16[2,768,2048]{2,1,0:T(8,128)(2,1)S(1)} %dispatch.1, bf16[1,2048,448]{1,2,0:T(8,128)(2,1)S(1)} %copy-done), kind=kOutput, calls=%fused_computation.9 | convolution fusion | flops 1409286144 | bytes 6356992 | tf_op jit(solution)/shard_map/dot_general | solution.py:451
  45.3 0.0 copy-done.4
  45.4 0.0 copy-start.3
  45.4 1.7 %fusion.10 = f32[768,448]{0,1:T(8,128)S(1)} fusion(bf16[2,768,2048]{2,1,0:T(8,128)(2,1)S(1)} %dispatch.1, bf16[1,2048,448]{1,2,0:T(8,128)(2,1)S(1)} %copy-done.4), kind=kOutput, calls=%fused_computation.11 | convolution fusion | flops 1409286144 | bytes 6356992 | tf_op jit(solution)/shard_map/dot_general | solution.py:452
  47.0 0.0 copy-done.3
  47.0 2.0 %multiply_convert_fusion.1 = (bf16[768,448]{0,1:T(8,128)(2,1)S(1)}, bf16[768,448]{0,1:T(8,128)(2,1)S(1)}) fusion(f32[768,448]{0,1:T(8,128)S(1)} %fusion.8, f32[768,448]{0,1:T(8,128)S(1)} %fusion.10, bf16[1,448,2048]{2,1,0:T(8,128)(2,1)S(1)} %copy-done.3, bf16[2,768,2048]{2,1,0:T(8,128)(2,1)S(1)} %dispatch.1), kind=kOutput, calls=%fused_computation.32 | convolution fusion | flops 1413758976 | bytes 9109504 | tf_op jit(solution)/shard_map/dot_general | solution.py:22
  49.1 2.9 %fusion.23 = bf16[1,448,2048]{2,1,0:T(8,128)(2,1)} fusion(bf16[2,768,2048]{2,1,0:T(8,128)(2,1)S(1)} %dispatch.1, f32[768,448]{0,1:T(8,128)S(1)} %fusion.10, f32[768,448]{0,1:T(8,128)S(1)} %fusion.8), kind=kOutput, calls=%fused_computation.18 | convolution fusion | flops 1412268032 | bytes 7733248 | tf_op jit(solution)/shard_map/dot_general | solution.py:18
  52.0 2.9 %fusion.29 = bf16[1,2048,448]{1,2,0:T(8,128)(2,1)} fusion(bf16[768,448]{0,1:T(8,128)(2,1)S(1)} %get-tuple-element.15, bf16[2,768,2048]{2,1,0:T(8,128)(2,1)S(1)} %dispatch.1), kind=kOutput, calls=%fused_computation.20 | convolution fusion | flops 1410203648 | bytes 5668864 | tf_op jit(solution)/shard_map/dot_general | solution.py:18
  54.8 2.9 %fusion.26 = bf16[1,2048,448]{1,2,0:T(8,128)(2,1)} fusion(bf16[768,448]{0,1:T(8,128)(2,1)S(1)} %get-tuple-element.16, bf16[2,768,2048]{2,1,0:T(8,128)(2,1)S(1)} %dispatch.1), kind=kOutput, calls=%fused_computation.19 | convolution fusion | flops 1410203648 | bytes 5668864 | tf_op jit(solution)/shard_map/dot_general | solution.py:18
  57.7 1.8 %fusion.36 = f32[768,2048]{1,0:T(8,128)S(1)} fusion(bf16[768,448]{0,1:T(8,128)(2,1)S(1)} %get-tuple-element.16, bf16[1,2048,448]{1,2,0:T(8,128)(2,1)S(1)} %copy-done), kind=kOutput, calls=%fused_computation.25 | convolution fusion | flops 1409286144 | bytes 8814592 | tf_op jit(solution)/shard_map/dot_general | solution.py:22
  59.5 3.7 %add_convert_fusion.grad_ref = bf16[768,2048]{1,0:T(8,128)(2,1)} fusion(f32[768,2048]{1,0:T(8,128)S(1)} %fusion.36, bf16[768,448]{0,1:T(8,128)(2,1)S(1)} %get-tuple-element.15, bf16[1,2048,448]{1,2,0:T(8,128)(2,1)S(1)} %copy-done.4), kind=kOutput, calls=%fused_computation | convolution fusion | flops 1412431872 | bytes 11960320 | tf_op jit(solution)/shard_map/dot_general | solution.py:22
  63.2 47.7 %tail.1 = (bf16[128,512]{1,0:T(8,128)(2,1)}, f32[256,128]{1,0:T(8,128)}, bf16[128,128]{1,0:T(8,128)(2,1)}, bf16[128,128]{1,0:T(8,128)(2,1)}) custom-call(bf16[768,2048]{1,0:T(8,128)(2,1)} %add_convert_fusion.grad_ref, s32[4,128]{1,0:T(4,128)} %copy-done.2, bf16[128,512]{1,0:T(8,128)(2,1)} %copy-done.1, bf16[128,128]{1,0:T(8,128)(2,1)} %value_ref.1, ...), custom_call_target="tpu_custom_call" | custom-call | tf_op jit(solution)/shard_map/tail/pallas_call | solution.py:400
  110.9 1.6 %copy.29 = bf16[128,512]{1,0:T(8,128)(2,1)} copy(bf16[128,512]{1,0:T(8,128)(2,1)} %get-tuple-element.29) | data formatting | bytes 262144
  112.5 1.6 %copy.30 = f32[256,128]{1,0:T(8,128)} copy(f32[256,128]{1,0:T(8,128)} %get-tuple-element.30) | data formatting | bytes 262144
  114.1 1.4 %copy.31 = bf16[128,128]{1,0:T(8,128)(2,1)} copy(bf16[128,128]{1,0:T(8,128)(2,1)} %get-tuple-element.31) | data formatting | bytes 65536
  115.5 1.4 %copy.32 = bf16[128,128]{1,0:T(8,128)(2,1)} copy(bf16[128,128]{1,0:T(8,128)(2,1)} %get-tuple-element.32) | data formatting | bytes 65536
Async XLA Ops:
  0.6 43.0 %copy-start = (bf16[1,2048,448]{1,2,0:T(8,128)(2,1)S(1)}, bf16[1,2048,448]{1,2,0:T(8,128)(2,1)}, u32[]{:S(2)}) copy-start(bf16[1,2048,448]{1,2,0:T(8,128)(2,1)} %param.18) | copy-start | bytes 5505028
  1.6 42.0 %copy-start.2 = (s32[4,128]{1,0:T(4,128)}, s32[4,128]{1,0:T(4,128)S(1)}, u32[]{:S(2)}) copy-start(s32[4,128]{1,0:T(4,128)S(1)} %fusion.43.rank_ref) | copy-start | bytes 6148
  4.7 39.0 %copy-start.1 = (bf16[128,512]{1,0:T(8,128)(2,1)}, bf16[128,512]{1,0:T(8,128)(2,1)S(1)}, u32[]{:S(2)}) copy-start(bf16[128,512]{1,0:T(8,128)(2,1)S(1)} %get-tuple-element.17.c_ref.cot_ref) | copy-start | bytes 393220
  43.7 1.7 %copy-start.4 = (bf16[1,2048,448]{1,2,0:T(8,128)(2,1)S(1)}, bf16[1,2048,448]{1,2,0:T(8,128)(2,1)}, u32[]{:S(2)}) copy-start(bf16[1,2048,448]{1,2,0:T(8,128)(2,1)} %param.19) | copy-start | bytes 5505028
  45.4 1.7 %copy-start.3 = (bf16[1,448,2048]{2,1,0:T(8,128)(2,1)S(1)}, bf16[1,448,2048]{2,1,0:T(8,128)(2,1)}, u32[]{:S(2)}) copy-start(bf16[1,448,2048]{2,1,0:T(8,128)(2,1)} %param.20) | copy-start | bytes 5505028

commit v2 on v1

--- a/solution.py
+++ b/solution.py
@@ -50,129 +50,14 @@
     return jnp.where(slots == rank_row, 1.0, 0.0)
 
 
-def dispatch_kernel(experts, cap, h_ref, c_ref, rank_ref, w_ref, out_ref, pack, z_send, z_recv, g_send, g_recv):
-    s, t, e, g, hi, lo, across, beside, partner = place()
-    quarter = h_ref.shape[1]
-    across_t = across[1]
-
-    def loc(j, side, col):
-        src = lax.rem(e + experts - j, experts)
-        rows = pl.ds(pl.multiple_of((src * GROUP + side) * cap, cap), cap)
-        cols = pl.ds(pl.multiple_of(col * quarter, quarter), quarter)
-        return rows, cols
-
-    z_peers = [(lax.rem(e + j, experts) * GROUP + g, t) for j in range(1, experts)]
-    greet(z_peers + [across, beside, partner])
-    sent = []
-    own_rows, own_cols = loc(0, g, t)
-    for j in list(range(1, experts)) + [0]:
-        target = lax.rem(e + j, experts)
-        rank_row = rank_ref[pl.ds(target, 1), :]
-        hot = one_hot(rank_row, cap)
-        scale = jnp.sum(hot * w_ref[pl.ds(target, 1), :], axis=1, keepdims=True)
-        hot = hot.astype(BF16)
-        rows = jnp.dot(hot, h_ref[...], preferred_element_type=F32).astype(BF16)
-        cots = (jnp.dot(hot, c_ref[...], preferred_element_type=F32) * scale).astype(BF16)
-        if j:
-            pack[j, 0] = rows
-            pack[j, 1] = cots
-            copy = remote(
-                pack.at[j], out_ref.at[:, own_rows, own_cols], z_send.at[j], z_recv.at[j], z_peers[j - 1]
-            )
-            copy.start()
-            sent.append(copy)
-        else:
-            out_ref[0, own_rows, own_cols] = rows
-            out_ref[1, own_rows, own_cols] = cots
-
-    def hop(n, j, ref, device):
-        return remote(ref, ref, g_send.at[j, n], g_recv.at[j, n], device)
-
-    def send(n, j, ref, device):
-        copy = hop(n, j, ref, device)
-        copy.start()
-        sent.append(copy)
-
-    def full(j, side, col):
-        rows, cols = loc(j, side, col)
-        return out_ref.at[:, rows, cols]
-
-    def part(k, j, side, col):
-        rows, cols = loc(j, side, col)
-        return out_ref.at[k, rows, cols]
-
-    def arrived(n, j, ref):
-        hop(n, j, ref, partner).wait_recv()
-
-    def first(j):
-        if j:
-            block = full(j, g, t)
-            remote(block, block, z_send.at[j], z_recv.at[j], partner).wait_recv()
-        block = full(j, g, t)
-        send(0, j, block, across)
-        send(1, j, block, beside)
-        send(2, j, block, partner)
-
-    def second(j):
-        arrived(0, j, full(j, g, across_t))
-        send(3, j, part(0, j, g, across_t), beside)
-        send(5, j, full(j, g, across_t), partner)
-        arrived(1, j, full(j, 1 - g, t))
-        send(4, j, part(1, j, 1 - g, t), across)
-        send(6, j, full(j, 1 - g, t), partner)
-
-    def third(j):
-        arrived(3, j, part(0, j, 1 - g, across_t))
-        send(7, j, part(0, j, 1 - g, across_t), partner)
-        arrived(4, j, part(1, j, 1 - g, across_t))
-        send(8, j, part(1, j, 1 - g, across_t), partner)
-
-    for j in range(experts + 2):
-        if j < experts:
-            first(j)
-        if 0 <= j - 1 < experts:
-            second(j - 1)
-        if 0 <= j - 2:
-            third(j - 2)
-    other_t = partner[1]
-    far_t = (1 - hi) * PAIR + 1 - lo
-    for j in range(experts):
-        arrived(2, j, full(j, g, other_t))
-        arrived(5, j, full(j, g, far_t))
-        arrived(6, j, full(j, 1 - g, other_t))
-        arrived(7, j, part(0, j, 1 - g, far_t))
-        arrived(8, j, part(1, j, 1 - g, far_t))
-    for copy in sent:
-        copy.wait_send()
-
-
-def dispatch(h_part, c_part, rank, weight, experts, cap, rows, width):
-    vmem = pl.BlockSpec(memory_space=pltpu.VMEM)
-    quarter = h_part.shape[1]
-    return pl.pallas_call(
-        functools.partial(dispatch_kernel, experts, cap),
-        out_shape=jax.ShapeDtypeStruct((2, rows, width), BF16),
-        in_specs=[vmem] * 4,
-        out_specs=vmem,
-        scratch_shapes=[
-            pltpu.VMEM((experts, 2, cap, quarter), BF16),
-            pltpu.SemaphoreType.DMA((experts,)),
-            pltpu.SemaphoreType.DMA((experts,)),
-            pltpu.SemaphoreType.DMA((experts, 9)),
-            pltpu.SemaphoreType.DMA((experts, 9)),
-        ],
-        compiler_params=pltpu.CompilerParams(
-            collective_id=0, has_side_effects=True, vmem_limit_bytes=40 * 1024 * 1024
-        ),
-        name="dispatch",
-    )(h_part, c_part, rank, weight)
-
-
-def tail_kernel(
+def mega_kernel(
     experts, cap, ksize,
-    grad_ref, rank_ref, cot_ref, value_ref, gate_ref, normed_ref, std_ref, gain_ref, taps_ref, proj_ref,
-    stream_ref, pgrad_ref, vgrad_ref, ggrad_ref,
+    h_ref, cot_ref, rank_ref, w_ref, gate_hbm, up_hbm, down_hbm,
+    value_ref, gate_ref, normed_ref, std_ref, gain_ref, taps_ref, proj_ref,
+    gw_hbm, uw_hbm, dw_hbm, stream_ref, pgrad_ref, vgrad_ref, ggrad_ref,
+    buf, pack, wg, wu, wd, act, gg, ug, grad_ref, gw, uw, dw,
     from_core, sums, rx_a, ry_b, relay, rx2, back, done, full, stats, ext, pg, py, pz_out, pz,
+    w_sem, o_sem, d_send, d_recv, g_send, g_recv,
     core_send, core_recv, hop_send, hop_recv, z_send, z_recv, t_send, t_recv, p_send, p_recv, q_send, q_recv,
 ):
     s, t, e, g, hi, lo, across, beside, partner = place()
@@ -180,38 +65,153 @@
     tok, quarter = cot_ref.shape
     half = quarter // 2
     tp_ways = stats.shape[0]
+    across_t, other_t = across[1], partner[1]
+    far_t = (1 - hi) * PAIR + 1 - lo
+    far = (s, far_t)
     z_peers = [(lax.rem(e + j, experts) * GROUP + g, t) for j in range(1, experts)]
-    far = (s, (1 - hi) * PAIR + 1 - lo)
     before = (lax.rem(s + sp_ways - 1, sp_ways), t)
     after = (lax.rem(s + 1, sp_ways), t)
-    greet(z_peers + [across, beside, partner, far, before, after])
+    loads = [
+        pltpu.make_async_copy(src, dst, w_sem.at[n])
+        for n, (src, dst) in enumerate(((gate_hbm, wg), (up_hbm, wu), (down_hbm, wd)))
+    ]
+    for copy in loads:
+        copy.start()
     sent = []
 
     def go(copy):
         copy.start()
         sent.append(copy)
 
-    order = list(range(1, experts)) + [0]
-
-    def rows_of(j):
-        target = lax.rem(e + j, experts)
-        return pl.ds(pl.multiple_of(target * GROUP * cap, cap), GROUP * cap)
-
     def cols_of(col):
         return pl.ds(pl.multiple_of(col * quarter, quarter), quarter)
+
+    def source_of(j):
+        return lax.rem(e + experts - j, experts)
+
+    def rows_of(j):
+        return pl.ds(pl.multiple_of(source_of(j) * GROUP * cap, cap), GROUP * cap)
+
+    def loc(j, side, col):
+        return pl.ds(pl.multiple_of((source_of(j) * GROUP + side) * cap, cap), cap), cols_of(col)
+
+    own_rows, own_cols = loc(0, g, t)
+
+    def d_copy(j):
+        return remote(pack.at[j], buf.at[:, own_rows, own_cols], d_send.at[j], d_recv.at[j], z_peers[j - 1])
+
+    greeted = False
+    for j in list(range(1, experts)) + [0]:
+        target = lax.rem(e + j, experts)
+        hot = one_hot(rank_ref[pl.ds(target, 1), :], cap)
+        scale = jnp.sum(hot * w_ref[pl.ds(target, 1), :], axis=1, keepdims=True)
+        hot = hot.astype(BF16)
+        rows = jnp.dot(hot, h_ref[...], preferred_element_type=F32).astype(BF16)
+        cots = (jnp.dot(hot, cot_ref[...], preferred_element_type=F32) * scale).astype(BF16)
+        if j:
+            pack[j, 0] = rows
+            pack[j, 1] = cots
+            if not greeted:
+                greet(z_peers + [across, beside, partner, far, before, after])
+                greeted = True
+            go(d_copy(j))
+        else:
+            buf[0, own_rows, own_cols] = rows
+            buf[1, own_rows, own_cols] = cots
+
+    def hop(n, j, ref, device):
+        return remote(ref, ref, g_send.at[j, n], g_recv.at[j, n], device)
+
+    def both(j, side, col):
+        rows, cols = loc(j, side, col)
+        return buf.at[:, rows, cols]
+
+    def one_of(k, j, side, col):
+        rows, cols = loc(j, side, col)
+        return buf.at[k, rows, cols]
+
+    def arrived(n, j, ref):
+        hop(n, j, ref, partner).wait_recv()
+
+    def d_first(j):
+        block = both(j, g, t)
+        if j:
+            remote(block, block, d_send.at[j], d_recv.at[j], partner).wait_recv()
+        go(hop(0, j, block, across))
+        go(hop(1, j, block, beside))
+        go(hop(2, j, block, partner))
+
+    def d_second(j):
+        arrived(0, j, both(j, g, across_t))
+        go(hop(3, j, one_of(0, j, g, across_t), beside))
+        go(hop(5, j, both(j, g, across_t), partner))
+        arrived(1, j, both(j, 1 - g, t))
+        go(hop(4, j, one_of(1, j, 1 - g, t), across))
+        go(hop(6, j, both(j, 1 - g, t), partner))
+
+    def d_third(j):
+        arrived(3, j, one_of(0, j, 1 - g, across_t))
+        go(hop(7, j, one_of(0, j, 1 - g, across_t), partner))
+        arrived(4, j, one_of(1, j, 1 - g, across_t))
+        go(hop(8, j, one_of(1, j, 1 - g, across_t), partner))
+
+    def d_last(j):
+        arrived(2, j, both(j, g, other_t))
+        arrived(5, j, both(j, g, far_t))
+        arrived(6, j, both(j, 1 - g, other_t))
+        arrived(7, j, one_of(0, j, 1 - g, far_t))
+        arrived(8, j, one_of(1, j, 1 - g, far_t))
+
+    def compute(j):
+        rows = rows_of(j)
+        in_rows = buf[0, rows, :]
+        in_cots = buf[1, rows, :]
+        pre_gate = jnp.dot(in_rows, wg[...], preferred_element_type=F32)
+        pre_up = jnp.dot(in_rows, wu[...], preferred_element_type=F32)
+        gate_sig = jax.nn.sigmoid(pre_gate)
+        silu_gate = pre_gate * gate_sig
+        act_grad = dot_cols(in_cots, wd[...])
+        gate_grad = (act_grad * pre_up * gate_sig * (1.0 + pre_gate * (1.0 - gate_sig))).astype(BF16)
+        up_grad = (act_grad * silu_gate).astype(BF16)
+        act[rows, :] = (silu_gate * pre_up).astype(BF16)
+        gg[rows, :] = gate_grad
+        ug[rows, :] = up_grad
+        grad_ref[rows, :] = (dot_cols(gate_grad, wg[...]) + dot_cols(up_grad, wu[...])).astype(BF16)
+
+    width = full.shape[1]
+    piece = 256
+    per_item = width // piece // 4
+
+    def weight_item(which, n):
+        @pl.loop(n * per_item, (n + 1) * per_item)
+        def _(i):
+            cols = pl.ds(pl.multiple_of(i * piece, piece), piece)
+            if which == 0:
+                gw[cols, :] = dot_rows(buf[0, :, cols], gg[...]).astype(BF16)
+            elif which == 1:
+                uw[cols, :] = dot_rows(buf[0, :, cols], ug[...]).astype(BF16)
+            else:
+                dw[:, cols] = dot_rows(act[...], buf[1, :, cols]).astype(BF16)
+
+    stores = [
+        pltpu.make_async_copy(src, dst, o_sem.at[n])
+        for n, (src, dst) in enumerate(((gw, gw_hbm), (uw, uw_hbm), (dw, dw_hbm)))
+    ]
+    items = [(which, n) for which in range(3) for n in range(4)]
+
+    def fill(count=1):
+        for _ in range(count):
+            if items:
+                which, n = items.pop(0)
+                weight_item(which, n)
+                if n == 3:
+                    stores[which].start()
 
     def core_copy(j, h, lane):
         return remote(
             grad_ref.at[rows_of(j), cols_of(h * PAIR + lane)],
-            from_core.at[j, h],
-            core_send.at[j, h],
-            core_recv.at[j, h],
-            partner,
+            from_core.at[j, h], core_send.at[j, h], core_recv.at[j, h], partner,
         )
-
-    for j in order:
-        for h in range(PAIR):
-            go(core_copy(j, h, 1 - lo))
 
     def hop_copy(n, j, src, dst, device):
         return remote(src, dst, hop_send.at[j, n], hop_recv.at[j, n], device)
@@ -229,7 +229,7 @@
         return hop_copy(3, j, relay.at[1, j], rx2.at[1, j], across)
 
     def z_copy(j):
-        return remote(done.at[j], back.at[j], z_send.at[j], z_recv.at[j], z_peers[j - 1])
+        return remote(done.at[j], back.at[j], z_send.at[j], z_recv.at[j], (source_of(j) * GROUP + g, t))
 
     def first(j):
         for h in range(PAIR):
@@ -261,13 +261,42 @@
         if j:
             go(z_copy(j))
 
-    for i in range(experts + 2):
+    step = max(1, experts // 4)
+    chunks = [list(range(c, min(c + step, experts))) for c in range(0, experts, step)]
+
+    def returns(c, fills):
+        for stage, lag in ((first, 1), (second, 2), (third, 3)):
+            if 0 <= c - lag < len(chunks):
+                for j in chunks[c - lag]:
+                    stage(j)
+                fill(fills)
+
+    for i in range(experts + 3):
         if i < experts:
-            first(order[i])
+            d_first(i)
         if 0 <= i - 1 < experts:
-            second(order[i - 1])
-        if 0 <= i - 2:
-            third(order[i - 2])
+            d_second(i - 1)
+        if 0 <= i - 2 < experts:
+            d_third(i - 2)
+        j = i - 3
+        if j >= 0:
+            if j == 0:
+                for copy in loads:
+                    copy.wait()
+            d_last(j)
+            if j % step == step - 1 or j == experts - 1:
+                c = j // step
+                if len(chunks[c]) == 1:
+                    compute(j)
+                else:
+                    pl.loop(chunks[c][0], chunks[c][-1] + 1)(compute)
+                for k in chunks[c]:
+                    for h in range(PAIR):
+                        go(core_copy(k, h, 1 - lo))
+                returns(c, 1 if c == len(chunks) - 1 else 0)
+    for c in range(len(chunks), len(chunks) + 3):
+        returns(c, 1)
+    fill(len(items))
 
     gain = gain_ref[...]
     saved = normed_ref[...].astype(F32)
@@ -283,7 +312,7 @@
             block = back[j]
         else:
             block = done[0]
-        source = lax.rem(e + experts - j, experts)
+        source = lax.rem(e + j, experts)
         hot = one_hot(rank_ref[pl.ds(source, 1), :], cap).astype(BF16)
         stream = stream + dot_rows(hot, block)
     stream = stream.astype(BF16)
@@ -350,7 +379,7 @@
 
     for i in range(experts):
         p_copy(i).wait_recv()
-    for j in order:
+    for j in list(range(1, experts)) + [0]:
         target = lax.rem(e + j, experts)
         piece = pg[target, g].astype(F32) + py[target].astype(F32)
         if j:
@@ -386,28 +415,47 @@
 
     for copy in sent:
         copy.wait_send()
-
-
-def tail(grad, rank, cot, value, gate_in, normed, std, gain, taps, w_proj, experts, cap, tp_ways):
+    for copy in stores:
+        copy.wait()
+
+
+def mega(h_part, rank, weight, w_gate, w_up, w_down, cot, value, gate_in, normed, std, gain, taps, w_proj, experts, cap, tp_ways):
     vmem = pl.BlockSpec(memory_space=pltpu.VMEM)
+    hbm = pl.BlockSpec(memory_space=pl.ANY)
     tok, quarter = cot.shape
-    width = grad.shape[1]
+    width, hidden = w_gate.shape
+    total = experts * GROUP * cap
     ch = normed.shape[1]
     rows = width // (experts * GROUP)
     half = quarter // 2
     dma = pltpu.SemaphoreType.DMA
-    assert ksize_ok(taps.shape[0])
+    assert taps.shape[0] - 1 <= 32
     return pl.pallas_call(
-        functools.partial(tail_kernel, experts, cap, taps.shape[0]),
+        functools.partial(mega_kernel, experts, cap, taps.shape[0]),
         out_shape=(
+            jax.ShapeDtypeStruct((width, hidden), BF16),
+            jax.ShapeDtypeStruct((width, hidden), BF16),
+            jax.ShapeDtypeStruct((hidden, width), BF16),
             jax.ShapeDtypeStruct((tok, quarter), BF16),
             jax.ShapeDtypeStruct((rows, ch), F32),
             jax.ShapeDtypeStruct((tok, ch), BF16),
             jax.ShapeDtypeStruct((tok, ch), BF16),
         ),
-        in_specs=[vmem] * 10,
-        out_specs=(vmem,) * 4,
+        in_specs=[vmem] * 4 + [hbm] * 3 + [vmem] * 7,
+        out_specs=(hbm,) * 3 + (vmem,) * 4,
         scratch_shapes=[
+            pltpu.VMEM((2, total, width), BF16),
+            pltpu.VMEM((experts, 2, cap, quarter), BF16),
+            pltpu.VMEM((width, hidden), BF16),
+            pltpu.VMEM((width, hidden), BF16),
+            pltpu.VMEM((hidden, width), BF16),
+            pltpu.VMEM((total, hidden), BF16),
+            pltpu.VMEM((total, hidden), BF16),
+            pltpu.VMEM((total, hidden), BF16),
+            pltpu.VMEM((total, width), BF16),
+            pltpu.VMEM((width, hidden), BF16),
+            pltpu.VMEM((width, hidden), BF16),
+            pltpu.VMEM((hidden, width), BF16),
             pltpu.VMEM((experts, PAIR, GROUP * cap, quarter), BF16),
             pltpu.VMEM((2, experts, PAIR, GROUP, cap, half), BF16),
             pltpu.VMEM((experts, GROUP, cap, half), BF16),
@@ -423,6 +471,12 @@
             pltpu.VMEM((experts, rows, ch), BF16),
             pltpu.VMEM((experts, rows, ch), BF16),
             pltpu.VMEM((experts, rows, ch), BF16),
+            dma((3,)),
+            dma((3,)),
+            dma((experts,)),
+            dma((experts,)),
+            dma((experts, 9)),
+            dma((experts, 9)),
             dma((experts, PAIR)),
             dma((experts, PAIR)),
             dma((experts, 4)),
@@ -437,30 +491,10 @@
             dma((experts,)),
         ],
         compiler_params=pltpu.CompilerParams(
-            collective_id=1, has_side_effects=True, vmem_limit_bytes=56 * 1024 * 1024
+            collective_id=0, has_side_effects=True, vmem_limit_bytes=56 * 1024 * 1024
         ),
-        name="tail",
-    )(grad, rank, cot, value, gate_in, normed, std, gain, taps, w_proj)
-
-
-def ksize_ok(taps):
-    return taps - 1 <= 32
-
-
-def expert_backward(in_rows, in_cots, gate_slice, up_slice, down_slice):
-    pre_gate = jnp.dot(in_rows, gate_slice, preferred_element_type=F32)
-    pre_up = jnp.dot(in_rows, up_slice, preferred_element_type=F32)
-    gate_sig = jax.nn.sigmoid(pre_gate)
-    silu_gate = pre_gate * gate_sig
-    act_rows = (silu_gate * pre_up).astype(BF16)
-    act_grad = dot_cols(in_cots, down_slice)
-    gate_grad = (act_grad * pre_up * gate_sig * (1.0 + pre_gate * (1.0 - gate_sig))).astype(BF16)
-    up_grad = (act_grad * silu_gate).astype(BF16)
-    row_grad = (dot_cols(gate_grad, gate_slice) + dot_cols(up_grad, up_slice)).astype(BF16)
-    down_grad = dot_rows(act_rows, in_cots).astype(BF16)
-    gate_wgrad = dot_rows(in_rows, gate_grad).astype(BF16)
-    up_wgrad = dot_rows(in_rows, up_grad).astype(BF16)
-    return gate_wgrad, up_wgrad, down_grad, row_grad
+        name="mega",
+    )(h_part, cot, rank, weight, w_gate, w_up, w_down, value, gate_in, normed, std, gain, taps, w_proj)
 
 
 def on_device(
@@ -484,11 +518,9 @@
     rank = jnp.where(named, rank, -1)
     h_part = lax.dynamic_slice_in_dim(hidden_state, offset, quarter, 1)
     c_part = lax.dynamic_slice_in_dim(out_grad, offset, quarter, 1)
-    got = dispatch(h_part, c_part, rank, weight, experts, cap, sp_ways * cap, width)
-    gate_wgrad, up_wgrad, down_grad, row_grad = expert_backward(got[0], got[1], w_gate[0], w_up[0], w_down[0])
-    stream_part, proj_grad, value_grad, gate_in_grad = tail(
-        row_grad, rank, c_part, value, gate_in, normed, inv_std[:, None], norm_gain[None, :], taps, w_proj,
-        experts, cap, tp_ways,
+    gate_wgrad, up_wgrad, down_grad, stream_part, proj_grad, value_grad, gate_in_grad = mega(
+        h_part, rank, weight, w_gate[0], w_up[0], w_down[0], c_part, value, gate_in, normed,
+        inv_std[:, None], norm_gain[None, :], taps, w_proj, experts, cap, tp_ways,
     )
     return gate_wgrad[None], up_wgrad[None], down_grad[None], stream_part, proj_grad, value_grad, gate_in_grad
 

time: 117 us -> 109 us (0.932)
  matrix products: 19.6 us -> 0.72 us
  local copies, waits for them, and re-layouts: 8.29 us -> 21.3 us
  Pallas kernels: 86.7 us -> 84.1 us
    dot_general x8 -> x0, matrix products: 19.5 us -> none  [the longest x3 8.61 us: dot_rows(): lax.dot_general(a, b, (((0,), (0,)), ((), ())), preferred_element_type=F32)]
    unnamed x14 -> x21, local copies, waits for them, and re-layouts: 5.91 us -> 18.2 us
    pallas_call x2 -> x1, Pallas kernels: 86.7 us -> 84.1 us  [mega(): pl.pallas_call(functools.partial(mega_kernel, experts, cap, taps.shape[0]...]
where the time goes in v2:
time: 109 us
  Pallas kernels  84.1 us (77%)
  local copies, waits for them, and re-layouts  21.3 us (20%)
  other arithmetic  1.98 us (2%)
    pallas_call x1, Pallas kernels, mega(): pl.pallas_call(functools.partial(mega_kernel, experts, cap, taps.shape[0]...  84.1 us
    unnamed x21, local copies, waits for them, and re-layouts  18.2 us

profile of v2, /device:TPU:0, one launch (start us, length us, event | category | flops | bytes accessed | tf_op | source)
XLA Modules:
  0.0 108.7 jit_solution(1198152891053707549)
XLA Ops:
  0.6 0.7 fusion.1
  1.3 0.7 fusion.rank_ref
  2.0 1.3 %select_reduce_fusion.w_ref = f32[4,128]{1,0:T(4,128)} fusion(f32[128,2]{0,1:T(2,128)} %param.17, s32[128,2]{0,1:T(2,128)} %param.16), kind=kLoop, calls=%fused_computation.3 | loop fusion | flops 2560 | bytes 4096 | tf_op jit(solution)/shard_map/reduce_sum | solution.py:514
  3.3 1.4 %copy.30.std_ref = f32[128,1]{1,0:T(8,128)} copy(f32[128,1]{0,1:T(1,128)} %bitcast.15) | data formatting | bytes 1024 | tf_op jit(solution)/shard_map/broadcast_in_dim | solution.py:523
  4.7 1.7 %constant_dynamic-slice_fusion = (bf16[128,512]{1,0:T(8,128)(2,1)}, bf16[128,512]{1,0:T(8,128)(2,1)}) fusion(bf16[128,2048]{1,0:T(8,128)(2,1)} %param.15, s32[]{:T(128)S(6)} %select_n.12, bf16[128,2048]{1,0:T(8,128)(2,1)} %param.14), kind=kLoop, calls=%fused_computation.6 | loop fusion | bytes 524292 | tf_op jit(solution)/shard_map/dynamic_slice | solution.py:520
  6.4 0.0 copy-start.1
  6.4 3.9 %copy.28 = bf16[1,2048,448]{2,1,0:T(8,128)(2,1)} copy(bf16[1,2048,448]{1,2,0:T(8,128)(2,1)} %param.18) | data formatting | bytes 3670016 | tf_op args[4]
  10.4 0.0 copy-done.1
  10.4 2.4 %copy.29 = bf16[1,2048,448]{2,1,0:T(8,128)(2,1)} copy(bf16[1,2048,448]{1,2,0:T(8,128)(2,1)S(1)} %copy-done.1) | data formatting | bytes 3670016 | tf_op args[5]
  12.8 84.1 %mega.1 = (bf16[2048,448]{1,0:T(8,128)(2,1)}, bf16[2048,448]{1,0:T(8,128)(2,1)}, bf16[448,2048]{1,0:T(8,128)(2,1)}, bf16[128,512]{1,0:T(8,128)(2,1)}, f32[256,12...) custom-call(bf16[128,512]{1,0:T(8,128)(2,1)} %get-tuple-element.36.h_ref, ...), custom_call_target="tpu_custom_call" | custom-call | tf_op jit(solution)/shard_map/mega/pallas_call | solution.py:433
  96.9 0.0 copy-start
  96.9 4.0 %copy.31 = bf16[1,2048,448]{1,2,0:T(8,128)(2,1)} copy(bf16[1,2048,448]{2,1,0:T(8,128)(2,1)} %bitcast.12) | data formatting | bytes 3670016
  100.9 0.0 copy-done
  100.9 2.3 %copy.32 = bf16[1,2048,448]{1,2,0:T(8,128)(2,1)} copy(bf16[1,2048,448]{2,1,0:T(8,128)(2,1)S(1)} %bitcast.11) | data formatting | bytes 3670016
  103.2 0.0 copy-start.3
  103.2 0.0 copy-start.2
  103.2 0.0 copy-start.5
  103.2 0.0 copy-start.4
  103.2 3.0 %copy.38 = bf16[1,448,2048]{2,1,0:T(8,128)(2,1)} copy(bf16[1,448,2048]{2,1,0:T(8,128)(2,1)} %bitcast.13) | data formatting | bytes 3670016
  106.2 0.0 copy-done.3
  106.2 0.7 copy.39
  106.9 0.0 copy-done.2
  106.9 0.7 copy.40
  107.5 0.0 copy-done.5
  107.5 0.6 copy.41
  108.1 0.0 copy-done.4
  108.1 0.6 copy.42
Async XLA Ops:
  6.4 4.0 %copy-start.1 = (bf16[1,2048,448]{1,2,0:T(8,128)(2,1)S(1)}, bf16[1,2048,448]{1,2,0:T(8,128)(2,1)}, u32[]{:S(2)}) copy-start(bf16[1,2048,448]{1,2,0:T(8,128)(2,1)} %param.19) | copy-start | bytes 5505028
  96.9 4.0 %copy-start = (bf16[2048,448]{1,0:T(8,128)(2,1)S(1)}, bf16[2048,448]{1,0:T(8,128)(2,1)}, u32[]{:S(2)}) copy-start(bf16[2048,448]{1,0:T(8,128)(2,1)} %get-tuple-element.15) | copy-start | bytes 5505028
  103.2 3.0 %copy-start.3 = (bf16[128,512]{1,0:T(8,128)(2,1)S(1)}, bf16[128,512]{1,0:T(8,128)(2,1)}, u32[]{:S(2)}) copy-start(bf16[128,512]{1,0:T(8,128)(2,1)} %get-tuple-element.47) | copy-start | bytes 393220
  103.2 3.7 %copy-start.2 = (f32[256,128]{1,0:T(8,128)S(1)}, f32[256,128]{1,0:T(8,128)}, u32[]{:S(2)}) copy-start(f32[256,128]{1,0:T(8,128)} %get-tuple-element.48) | copy-start | bytes 393220
  103.2 4.3 %copy-start.5 = (bf16[128,128]{1,0:T(8,128)(2,1)S(1)}, bf16[128,128]{1,0:T(8,128)(2,1)}, u32[]{:S(2)}) copy-start(bf16[128,128]{1,0:T(8,128)(2,1)} %get-tuple-element.49) | copy-start | bytes 98308
  103.2 4.9 %copy-start.4 = (bf16[128,128]{1,0:T(8,128)(2,1)S(1)}, bf16[128,128]{1,0:T(8,128)(2,1)}, u32[]{:S(2)}) copy-start(bf16[128,128]{1,0:T(8,128)(2,1)} %get-tuple-element.50) | copy-start | bytes 98308
